TPU v7x, 32 devices: a whole 2x2x4 slice. The times are simulated.
32 devices in a mesh: ep: 8 (over z, core), tp: 4 (over y, x).
Axes of the slice: x: 2, y: 2, z: 4, core: 2. Of those that a mesh axis runs over, the one named last changes fastest.
Arguments:
- receptance: bfloat16 [2048, 2048], P('ep', 'tp'), may hold values from -6 to 6
- key_tensor: bfloat16 [2048, 2048], P('ep', 'tp'), may hold values from -6 to 6
- value_tensor: bfloat16 [2048, 2048], P('ep', 'tp'), may hold values from -6 to 6
- decay_data_input: bfloat16 [2048, 2048], P('ep', 'tp'), may hold values from -4 to 4
- correction_rate_input: bfloat16 [2048, 2048], P('ep', 'tp'), may hold values from -16 to 6
- mixer_output_gate: bfloat16 [2048, 2048], P('ep', 'tp'), may hold values from -6 to 6
- decay_channel_offset: float32 [2048], P('tp'), may hold values from -16 to -3
- head_norm_gain: float32 [2048], P('tp'), may hold values from 0.1 to 1.9
- self_key_weight: float32 [2048], P('tp'), may hold values from -2 to 2
- mixer_output_weight: bfloat16 [2048, 2048], P('tp'), may hold values from -0.125 to 0.125
- second_batch_rows: bfloat16 [1024, 2048], P('ep'), may hold values from -6 to 6
- routed_expert_index: int32 [1024, 4], P('ep'), may hold values from 0 to 7, all different within a row; in each aligned block of 128 rows (0 to 127, 128 to 255, ...) at most 96 rows name the same one
- routing_output_weight: float32 [1024, 4], P('ep'), may hold values from 0.1 to 1
- expert_norm_gain: float32 [2048], replicated, may hold values from 0.1 to 1.9
- expert_gate_weight: bfloat16 [8, 1024, 2048], P('ep', 'tp'), may hold values from -0.125 to 0.125
- expert_up_weight: bfloat16 [8, 1024, 2048], P('ep', 'tp'), may hold values from -0.125 to 0.125
- expert_down_weight: bfloat16 [8, 1024, 2048], P('ep', None, 'tp'), may hold values from -0.1875 to 0.1875
- common_expert_gate: bfloat16 [1024, 2048], P('tp'), may hold values from -0.125 to 0.125
- common_expert_up: bfloat16 [1024, 2048], P('tp'), may hold values from -0.125 to 0.125
- common_expert_down: bfloat16 [1024, 2048], P(None, 'tp'), may hold values from -0.1875 to 0.1875
Outputs:
- token_mixer_output: bfloat16 [2048, 2048], P(('ep', 'tp'))
- expert_out: bfloat16 [1024, 2048], P('ep', 'tp')
Inputs may be any that keep to these rules, and one draw needn't show every extreme that they name: `routed_expert_index`: each row names 4 different experts. Within the rows of one index of ep no expert is named by more than 96 rows, and that bound is met in some index's rows.
All inputs are finite; a program needn't handle non-finite values.
Results may differ from a plain program's by a relative error of at most 0.017.
Values may be sent and summed in bfloat16 or wider, within the bound.
A program may use at most 128 MiB of HBM per device.

v0:
```python
import math
import jax
import jax.numpy as jnp
from jax import lax
from jax.sharding import PartitionSpec as P

HEAD_CHANNELS = 64
SPAN = 64
HIGHEST = lax.Precision.HIGHEST
PRECISION = lax.Precision.HIGH
NORM_FLOOR = 1.0


def head_view(matrix):
    return matrix.astype(jnp.float32).reshape(matrix.shape[0], -1, HEAD_CHANNELS)


def complete_head_outputs(
    state_readout,
    receptance_rows,
    key_row_block,
    value_row_block,
    head_norm_gain,
    self_key_weight,
    mixer_output_gate,
):
    mean_part = jnp.mean(state_readout, axis=-1, keepdims=True)
    spread = jnp.mean(jnp.square(state_readout - mean_part), axis=-1, keepdims=True)
    normalized_rows = (state_readout - mean_part) * lax.rsqrt(spread + NORM_FLOOR)
    sequence_length = state_readout.shape[0]
    normalized_rows = normalized_rows.reshape(sequence_length, -1) * head_norm_gain
    self_key_term = (
        jnp.sum(
            receptance_rows * key_row_block * self_key_weight.reshape(-1, HEAD_CHANNELS),
            axis=-1,
            keepdims=True,
        )
        * value_row_block
    )
    mixer_result = (
        normalized_rows + self_key_term.reshape(sequence_length, -1)
    ) * mixer_output_gate.astype(jnp.float32)
    return mixer_result.astype(jnp.bfloat16)


def product(spec, left, right):
    return jnp.einsum(spec, left, right, precision=PRECISION, preferred_element_type=jnp.float32)


def lower_inverse(strict, size):
    at = jnp.arange(size)
    row, column = (at[:, None], at[None, :])
    inverse = None
    block = 1
    while block < size:
        pair = (
            (row // (2 * block) == column // (2 * block))
            & (row // block % 2 == 1)
            & (column // block % 2 == 0)
        )
        below = jnp.where(pair, strict, 0.0)
        if inverse is None:
            inverse = jnp.eye(size, dtype=jnp.float32) - below
        else:
            inverse = inverse - product(
                "nhij,nhjk->nhik", product("nhij,nhjk->nhik", inverse, below), inverse
            )
        block *= 2
    return inverse


def mixer_part(
    receptance,
    key_tensor,
    value_tensor,
    decay_data_input,
    correction_rate_input,
    mixer_output_gate,
    decay_channel_offset,
    head_norm_gain,
    self_key_weight,
    mixer_output_weight,
):
    row_count, width = receptance.shape
    head_count = width // HEAD_CHANNELS
    span = min(SPAN, row_count)
    block_count = row_count // span
    receptance_rows = head_view(receptance)
    key_row_block = head_view(key_tensor)
    value_row_block = head_view(value_tensor)

    def by_block(matrix):
        return (
            matrix.astype(jnp.float32)
            .reshape(block_count, span, head_count, HEAD_CHANNELS)
            .transpose(0, 2, 1, 3)
        )

    step_log = -math.exp(-0.5) * jax.nn.sigmoid(
        decay_channel_offset + decay_data_input.astype(jnp.float32)
    )
    at = jnp.arange(span)
    reach = (at[:, None] >= at[None, :]).astype(jnp.float32)
    step_log = by_block(step_log)
    total_log = jnp.einsum("ts,nhsd->nhtd", reach, step_log, precision=HIGHEST)
    recept, keys, values = (by_block(receptance), by_block(key_tensor), by_block(value_tensor))
    units = keys * lax.rsqrt(jnp.sum(keys * keys, axis=-1, keepdims=True) + 1.0)
    corrections = units * jax.nn.sigmoid(by_block(correction_rate_input))
    grown = jnp.exp(-total_log)
    last_log = total_log[:, :, -1:, :]
    unit_in = units * jnp.exp(total_log - step_log)
    recept_in = recept * jnp.exp(total_log)
    tail = jnp.exp(last_log - total_log)
    scores = product(
        "nhtd,nhsd->nhts",
        jnp.concatenate([unit_in, recept_in], axis=2),
        jnp.concatenate([keys * grown, corrections * grown], axis=2),
    )
    before = at[:, None] > at[None, :]
    upto = at[:, None] >= at[None, :]
    unit_key = jnp.where(before, scores[:, :, :span, :span], 0.0)
    unit_fix = jnp.where(before, scores[:, :, :span, span:], 0.0)
    read_key = jnp.where(upto, scores[:, :, span:, :span], 0.0)
    read_fix = jnp.where(upto, scores[:, :, span:, span:], 0.0)
    inverse = lower_inverse(unit_fix, span)
    key_values = product("nhts,nhsd->nhtd", jnp.concatenate([unit_key, read_key], axis=2), values)
    solved = product(
        "nhts,nhsd->nhtd", inverse, jnp.concatenate([unit_in, key_values[:, :, :span]], axis=3)
    )
    reads = jnp.concatenate([recept_in, key_values[:, :, span:]], axis=3) - product(
        "nhts,nhsd->nhtd", read_fix, solved
    )
    eye_head = jnp.eye(HEAD_CHANNELS, dtype=jnp.float32)
    fresh = product("nhtj,nhti->nhji", keys * tail, values)
    moves = jnp.concatenate([eye_head * jnp.exp(last_log), fresh], axis=3) - product(
        "nhtj,nhti->nhji", corrections * tail, solved
    )
    whole = moves[0]
    for block in range(1, block_count):
        step = product("hij,hjk->hik", moves[block, :, :, :HEAD_CHANNELS], whole)
        whole = step + jnp.concatenate(
            [jnp.zeros_like(step[..., :HEAD_CHANNELS]), moves[block, :, :, HEAD_CHANNELS:]], axis=2
        )
    everything = lax.all_gather(whole.astype(jnp.bfloat16), "ep")
    mine = lax.axis_index("ep")
    state = jnp.zeros((head_count, HEAD_CHANNELS, HEAD_CHANNELS), jnp.float32)
    for k in range(lax.axis_size("ep") - 1):
        part = everything[k].astype(jnp.float32)
        new = product("hij,hjk->hik", part[..., :HEAD_CHANNELS], state)
        state = jnp.where(k < mine, new + part[..., HEAD_CHANNELS:], state)
    starts = [state]
    for block in range(block_count - 1):
        state = (
            product("hij,hjk->hik", moves[block, :, :, :HEAD_CHANNELS], state)
            + moves[block, :, :, HEAD_CHANNELS:]
        )
        starts.append(state)
    merged_output = reads[..., HEAD_CHANNELS:] + product(
        "nhtj,nhji->nhti", reads[..., :HEAD_CHANNELS], jnp.stack(starts)
    )
    merged_output = merged_output.transpose(0, 2, 1, 3).reshape(
        row_count, head_count, HEAD_CHANNELS
    )
    mixer_result = complete_head_outputs(
        merged_output,
        receptance_rows,
        key_row_block,
        value_row_block,
        head_norm_gain,
        self_key_weight,
        mixer_output_gate,
    )
    return lax.psum_scatter(
        jnp.dot(mixer_result, mixer_output_weight, preferred_element_type=jnp.float32).astype(
            jnp.bfloat16
        ),
        "tp",
        scatter_dimension=0,
        tiled=True,
    )


def activate(rows_in, gate_part, up_part):
    pre_gate = jnp.einsum("fd,rd->fr", gate_part, rows_in, preferred_element_type=jnp.float32)
    pre_up = jnp.einsum("fd,rd->fr", up_part, rows_in, preferred_element_type=jnp.float32)
    return (jax.nn.silu(pre_gate) * pre_up).astype(jnp.bfloat16)


def expert_entry(
    second_batch_rows,
    routed_expert_index,
    routing_output_weight,
    expert_norm_gain,
    common_expert_gate,
    common_expert_up,
):
    row_count, width = second_batch_rows.shape
    top_count = routed_expert_index.shape[1]
    peer_count = lax.axis_size("ep")
    slot_count = 3 * row_count * top_count // (2 * peer_count)
    widened = second_batch_rows.astype(jnp.float32)
    normalized_rows = (
        widened
        * lax.rsqrt(jnp.mean(widened * widened, axis=-1, keepdims=True) + NORM_FLOOR)
        * expert_norm_gain
    ).astype(jnp.bfloat16)
    flat_ids = routed_expert_index.reshape(-1)
    one_hot = (flat_ids[:, None] == jnp.arange(peer_count, dtype=jnp.int32)[None, :]).astype(
        jnp.int32
    )
    slot_rank = jnp.sum((jnp.cumsum(one_hot, axis=0) - 1) * one_hot, axis=1)
    target = flat_ids * slot_count + slot_rank
    owners = jnp.arange(row_count * top_count, dtype=jnp.int32) // top_count
    source_row = jnp.full((peer_count * slot_count,), row_count, jnp.int32).at[target].set(owners)
    padded = jnp.concatenate([normalized_rows, jnp.zeros((1, width), jnp.bfloat16)], axis=0)
    outgoing = jnp.take(padded, source_row, axis=0).reshape(peer_count, slot_count, width)
    shared_hidden = activate(normalized_rows, common_expert_gate, common_expert_up)
    piece_width = width // lax.axis_size("tp")
    own_slice = lax.dynamic_slice_in_dim(
        outgoing, lax.axis_index("tp") * piece_width, piece_width, 2
    )
    arrived = lax.all_to_all(own_slice, "ep", split_axis=0, concat_axis=0, tiled=True)
    return (arrived, shared_hidden, target)


def expert_exit(
    arrived,
    shared_hidden,
    target,
    routing_output_weight,
    expert_gate_weight,
    expert_up_weight,
    expert_down_weight,
    common_expert_down,
):
    peer_count, slot_count, piece_width = arrived.shape
    row_count, top_count = routing_output_weight.shape
    out_width = expert_down_weight.shape[2]
    flat_rows = arrived.reshape(-1, piece_width)
    pieces = lax.all_gather(flat_rows, "tp", axis=1, tiled=True)
    gate_cols = expert_gate_weight[0]
    up_cols = expert_up_weight[0]
    pre_gate = jnp.einsum("fd,rd->fr", gate_cols, pieces, preferred_element_type=jnp.float32)
    pre_up = jnp.einsum("fd,rd->fr", up_cols, pieces, preferred_element_type=jnp.float32)
    routed_hidden = (jax.nn.silu(pre_gate) * pre_up).astype(jnp.bfloat16)
    both = lax.all_gather(
        jnp.concatenate([routed_hidden, shared_hidden], axis=1), "tp", axis=0, tiled=True
    )
    pieces = (both[:, : routed_hidden.shape[1]], both[:, routed_hidden.shape[1] :])
    routed_rows = expert_down_weight[0]
    routed_sum = jnp.einsum("fr,fd->rd", pieces[0], routed_rows, preferred_element_type=jnp.float32)
    shared_out = jnp.einsum(
        "fr,fd->rd", pieces[1], common_expert_down, preferred_element_type=jnp.float32
    )
    returned = lax.all_to_all(
        routed_sum.astype(jnp.bfloat16).reshape(peer_count, slot_count, out_width),
        "ep",
        split_axis=0,
        concat_axis=0,
        tiled=True,
    )
    picked = jnp.take(returned.reshape(-1, out_width), target, axis=0).reshape(
        row_count, top_count, out_width
    )
    merged_output = (
        jnp.sum(picked.astype(jnp.float32) * routing_output_weight[:, :, None], axis=1) + shared_out
    )
    return merged_output.astype(jnp.bfloat16)


def on_device(
    receptance,
    key_tensor,
    value_tensor,
    decay_data_input,
    correction_rate_input,
    mixer_output_gate,
    decay_channel_offset,
    head_norm_gain,
    self_key_weight,
    mixer_output_weight,
    second_batch_rows,
    routed_expert_index,
    routing_output_weight,
    expert_norm_gain,
    expert_gate_weight,
    expert_up_weight,
    expert_down_weight,
    common_expert_gate,
    common_expert_up,
    common_expert_down,
):
    arrived, shared_hidden, target = expert_entry(
        second_batch_rows,
        routed_expert_index,
        routing_output_weight,
        expert_norm_gain,
        common_expert_gate,
        common_expert_up,
    )
    arrived, receptance, key_tensor, value_tensor, decay_data_input, correction_rate_input = (
        lax.optimization_barrier(
            (arrived, receptance, key_tensor, value_tensor, decay_data_input, correction_rate_input)
        )
    )
    token_mixer_output = mixer_part(
        receptance,
        key_tensor,
        value_tensor,
        decay_data_input,
        correction_rate_input,
        mixer_output_gate,
        decay_channel_offset,
        head_norm_gain,
        self_key_weight,
        mixer_output_weight,
    )
    expert_out = expert_exit(
        arrived,
        shared_hidden,
        target,
        routing_output_weight,
        expert_gate_weight,
        expert_up_weight,
        expert_down_weight,
        common_expert_down,
    )
    return (token_mixer_output, expert_out)


def solution(mesh):
    in_specs = (
        P("ep", "tp"),
        P("ep", "tp"),
        P("ep", "tp"),
        P("ep", "tp"),
        P("ep", "tp"),
        P("ep", "tp"),
        P("tp"),
        P("tp"),
        P("tp"),
        P("tp", None),
        P("ep", None),
        P("ep", None),
        P("ep", None),
        P(),
        P("ep", "tp", None),
        P("ep", "tp", None),
        P("ep", None, "tp"),
        P("tp", None),
        P("tp", None),
        P(None, "tp"),
    )
    out_specs = (P(("ep", "tp"), None), P("ep", "tp"))
    return jax.shard_map(
        on_device, mesh=mesh, in_specs=in_specs, out_specs=out_specs, check_vma=False
    )
```

profile of v0, /device:TPU:0, one launch (start us, length us, event | category | flops | bytes accessed | tf_op | source)
XLA Modules:
  0.0 244.3 jit_solution(18401035282546436214)
XLA Ops:
  7.2 0.8 broadcast_multiply_fusion.2
  9.3 1.1 reduce-window.6
  10.8 2.4 %scatter_custom_fusion = s32[768]{0:T(1024)S(1)} fusion(s32[512]{0:T(512)S(1)} %bitcast.192, s32[512]{0:T(512)S(1)} %add_select_fusion, s32[]{:T(128)} %constant.328.clone.1), kind=kCustom, calls=%fused_computation.208 | custom fusion | bytes 3076 | tf_op jit(solution)/shard_map/scatter | solution.py:214
  13.3 1.2 fusion.32
  14.6 1.2 fusion.34
  16.7 4.3 %gather_fusion = bf16[768,2048]{1,0:T(8,128)(2,1)} fusion(bf16[129,2048]{1,0:T(8,128)(2,1)S(1)} %concatenate.33, s32[1024]{0:T(1024)S(1)} %pad_clamp_fusion.1), kind=kCustom, calls=%fused_computation | custom fusion | bytes 6294528 | tf_op jit(solution)/shard_map/jit(_take)/gather | solution.py:216
  20.9 2.3 dynamic-slice_select_fusion
  23.2 6.4 %all-to-all-start = ((bf16[8,96,512]{2,1,0:T(8,128)(2,1)}), bf16[8,96,512]{2,1,0:T(8,128)(2,1)S(1)}, u32[]{:S(2)}, u32[]{:S(2)}) async-start(bf16[8,96,512]{2,1,0:T(8,128)(2,1)} %dynamic-slice_select_fusion), calls=%async_computation | async-start | bytes 1572864 | tf_op jit(solution)/shard_map/all_to_all | solution.py:222
  30.5 20.0 %all-to-all-done = bf16[8,96,512]{2,1,0:T(8,128)(2,1)S(1)} async-done(((bf16[8,96,512]{2,1,0:T(8,128)(2,1)}), bf16[8,96,512]{2,1,0:T(8,128)(2,1)S(1)}, u32[]{:S(2)}, u32[]{:S(2)}) %all-to-all-start) | async-done | bytes 786464 | tf_op jit(solution)/shard_map/all_to_all | solution.py:222
  50.7 1.9 copy.246
  52.6 2.3 add_divide_fusion
  54.9 2.2 reshape.842
  57.1 1.4 reshape.885
  58.6 1.6 copy.252
  60.5 2.2 reshape.834
  62.7 2.4 reshape.884
  65.1 2.6 %copy.248 = f32[4,64,8,64]{3,1,2,0:T(8,128)} copy(f32[4,64,8,64]{1,0,3,2:T(4,128)} %reshape.884) | data formatting | bytes 1048576 | tf_op jit(solution)/shard_map/reshape | solution.py:95
  67.7 5.0 %fusion.67 = (f32[4,8,64,64]{3,2,1,0:T(8,128)S(1)}, f32[4,8,64,64]{3,2,1,0:T(8,128)S(1)}, f32[4,8,64,64]{3,2,1,0:T(8,128)S(1)}, f32[4,8,64,64]{3,2,1,0:T(8,128)S(1)}, f32[4,8,64,64]{3,2,1,0:T(8,128)}) fusion(f32[4,64,8,64]{3,2,1,0:T(8,128)} %reshape.842, f32[4,8,64]{2,1,0:T(8,128)S(1)} %add_rsqrt_fusion.1, f32[4,64,8,64]{3,1,2,0:T(8,128)S(1)} %copy.252, ...), kind=kOutput, calls=%fused_computation.114 | convolution fusion | flops 101715968 | bytes 4726784 | tf_op jit(solution)/shard_map/ts,nhsd->nhtd/dot_general | solution.py:105
  72.7 2.3 fusion.1
  75.1 1.0 fusion.64
  76.1 0.9 convolution_subtract_fusion.4
  77.0 0.8 fusion.62
  78.5 0.8 fusion.60
  80.0 0.8 fusion.58
  80.9 0.9 convolution_subtract_fusion.1
  81.8 0.8 fusion.56
  82.6 1.6 convolution_subtract_fusion
  84.3 1.6 slice_select_fusion.4
  85.9 2.1 reshape.836
  87.9 2.5 %fusion.8 = f32[4,8,128,64]{3,2,1,0:T(8,128)S(1)} fusion(f32[4,8,64,64]{3,2,1,0:T(8,128)} %get-tuple-element.19, f32[4,8,64,64]{3,2,1,0:T(8,128)} %get-tuple-element.18, bf16[4,8,64,64]{3,1,2,0:T(8,128)(2,1)} %bitcast.178), kind=kOutput, calls=%fused_computation.12 | convolution fusion | flops 100925440 | bytes 2359296 | tf_op jit(solution)/shard_map/nhts,nhsd->nhtd/dot_general | solution.py:47
  90.4 1.1 fusion.129
  93.7 0.9 fusion.36
  94.9 1.7 convolution_subtract_fusion.5
  97.7 0.9 fusion.28
  99.6 1.7 convolution_bitcast_fusion.4
  101.3 2.0 fusion.31
  103.3 1.0 convert_multiply_fusion.2
  104.3 1.0 fusion
  105.2 2.0 copy.274
  107.3 3.7 %convolution_subtract_fusion.6 = f32[4,8,64,128]{3,2,1,0:T(8,128)} fusion(f32[4,8,64,128]{3,2,1,0:T(8,128)} %copy-done.8, f32[4,8,128,128]{3,2,1,0:T(8,128)} %copy-done.1, f32[4,8,64,64]{3,2,1,0:T(8,128)} %get-tuple-element.16, f32[4,8,64,64]{3,2,1,0:T(8,128)S(1)} %copy-done.7, pred[64,64]{1,0:T(8,128)(4,1)S(1)} %iota_compare_fusion.2), kind=kOutput, calls=%fused_computation.27 | convolution fusion | flops 101318656 | bytes 4722688 | tf_op jit(solution)/shard_map/nhts,nhsd->nhtd/dot_general | solution.py:47
  111.0 9.0 %all-gather.9.cloned.1.call-done = bf16[64,64,128]{2,1,0:T(8,128)(2,1)} async-done(((bf16[8,64,128]{2,1,0:T(8,128)(2,1)}), bf16[64,64,128]{2,1,0:T(8,128)(2,1)}) %all-gather.9.cloned.1.call-update) | async-done | bytes 1048592 | tf_op jit(solution)/shard_map/all_gather | solution.py:144
  120.0 1.2 fusion.27
  121.2 1.2 fusion.26
  122.4 1.2 fusion.25
  123.6 41.5 %all-gather.5.cloned.1.call-done = bf16[768,2048]{1,0:T(8,128)(2,1)} async-done(((bf16[768,512]{1,0:T(8,128)(2,1)}), bf16[768,2048]{1,0:T(8,128)(2,1)}) %all-gather.5.cloned.1.call-update) | async-done | bytes 3145744 | tf_op jit(solution)/shard_map/all_gather | solution.py:240
  165.1 3.3 %convolution_bitcast_fusion.2 = f32[256,768]{0,1:T(8,128)S(1)} fusion(bf16[768,2048]{1,0:T(8,128)(2,1)} %all-gather.5.cloned.1.call-done, bf16[1,256,2048]{2,1,0:T(8,128)(2,1)} %param.34), kind=kOutput, calls=%fused_computation.32 | convolution fusion | flops 805306368 | bytes 4980736 | tf_op jit(solution)/shard_map/fd,rd->fr/dot_general | solution.py:243
  168.5 1.0 fusion.19
  169.5 0.8 pad_maximum_fusion
  170.7 1.2 fusion.24
  171.9 1.3 fusion.23
  173.2 1.2 fusion.22
  174.4 1.2 fusion.21
  176.4 1.0 fusion.130
  178.8 0.8 mul.191
  179.6 2.1 copy.273
  181.7 1.1 reshape.837
  183.1 3.2 %convolution_convert_fusion = bf16[256,2048]{1,0:T(8,128)(2,1)} fusion(bf16[512,2048]{1,0:T(8,128)(2,1)S(1)} %copy-done, bf16[256,512]{1,0:T(8,128)(2,1)} %param.25, f32[256,512]{1,0:T(8,128)} %copy.274, bf16[256,512]{1,0:T(8,128)(2,1)S(1)} %copy-done.17, f32[256,512]{1,0:T(8,128)} %copy.273, f32[256,512]{1,0:T(8,128)} %reshape.837, ...), kind=kOutput, calls=%fused_computation.4 | convolution fusion | flops 538574848 | bytes 5769216 | tf_op jit(solution)/shard_map/dot_general | solution.py:174
  186.4 17.0 %all-gather.7.cloned.1.call-done = bf16[1024,896]{0,1:T(8,128)(2,1)} async-done(((bf16[256,896]{0,1:T(8,128)(2,1)}), bf16[1024,896]{0,1:T(8,128)(2,1)}) %all-gather.7.cloned.1.call-update) | async-done | bytes 1835024 | tf_op jit(solution)/shard_map/all_gather | solution.py:246
  203.4 3.5 %fusion.14 = bf16[768,512]{1,0:T(8,128)(2,1)} fusion(bf16[1024,896]{0,1:T(8,128)(2,1)} %all-gather.7.cloned.1.call-done, bf16[1,1024,512]{2,1,0:T(8,128)(2,1)} %param.36), kind=kOutput, calls=%fused_computation.23 | convolution fusion | flops 805699584 | bytes 3407872 | tf_op jit(solution)/shard_map/fr,fd->rd/dot_general | solution.py:251
  207.0 4.6 %all-to-all-start.1 = ((bf16[8,96,512]{2,1,0:T(8,128)(2,1)}), bf16[8,96,512]{2,1,0:T(8,128)(2,1)S(1)}, u32[]{:S(2)}, u32[]{:S(2)}) async-start(bf16[8,96,512]{2,1,0:T(8,128)(2,1)} %bitcast.187), calls=%async_computation.2 | async-start | bytes 1572864 | tf_op jit(solution)/shard_map/all_to_all | solution.py:255
  212.0 20.5 %all-to-all-done.1 = bf16[8,96,512]{2,1,0:T(8,128)(2,1)S(1)} async-done(((bf16[8,96,512]{2,1,0:T(8,128)(2,1)}), bf16[8,96,512]{2,1,0:T(8,128)(2,1)S(1)}, u32[]{:S(2)}, u32[]{:S(2)}) %all-to-all-start.1) | async-done | bytes 786464 | tf_op jit(solution)/shard_map/all_to_all | solution.py:255
  232.5 2.0 gather_fusion.1
  234.6 0.9 multiply_reduce_fusion
  235.5 2.3 fusion.29
  (131 shorter events, 12.9 us)
Async XLA Ops:
  7.2 175.9 %copy-start = (bf16[512,2048]{1,0:T(8,128)(2,1)S(1)}, bf16[512,2048]{1,0:T(8,128)(2,1)}, u32[]{:S(2)}) copy-start(bf16[512,2048]{1,0:T(8,128)(2,1)} %param.29) | copy-start | bytes 6291460
  15.8 0.8 copy-start.12
  20.9 29.6 %copy-start.18 = (bf16[256,512]{1,0:T(8,128)(2,1)S(1)}, bf16[256,512]{1,0:T(8,128)(2,1)}, u32[]{:S(2)}) copy-start(bf16[256,512]{1,0:T(8,128)(2,1)} %param.21) | copy-start | bytes 786436
  20.9 31.7 %copy-start.20 = (f32[512]{0:T(512)S(1)}, f32[512]{0:T(512)}, u32[]{:S(2)}) copy-start(f32[512]{0:T(512)} %param.26) | copy-start | bytes 6148
  23.2 27.3 %all-to-all-start = ((bf16[8,96,512]{2,1,0:T(8,128)(2,1)}), bf16[8,96,512]{2,1,0:T(8,128)(2,1)S(1)}, u32[]{:S(2)}, u32[]{:S(2)}) async-start(bf16[8,96,512]{2,1,0:T(8,128)(2,1)} %dynamic-slice_select_fusion), calls=%async_computation | async-start | bytes 1572864 | tf_op jit(solution)/shard_map/all_to_all | solution.py:222
  29.6 90.4 %all-gather.9.cloned.1.call-start = ((), (), s32[]{:S(2)}) async-start(), calls=%async_computation.6 | async-start | bytes 1179648 | tf_op jit(solution)/shard_map/all_gather | solution.py:144
  50.5 6.6 %copy-start.16 = (bf16[8,96,512]{2,1,0:T(8,128)(2,1)}, bf16[8,96,512]{2,1,0:T(8,128)(2,1)S(1)}, u32[]{:S(2)}) copy-start(bf16[8,96,512]{2,1,0:T(8,128)(2,1)S(1)} %all-to-all-done) | copy-start | bytes 2359300
  72.7 2.3 copy-start.6
  72.7 2.3 copy-start.9
  75.1 9.2 %copy-start.1 = (f32[4,8,128,128]{3,2,1,0:T(8,128)}, f32[4,8,128,128]{3,2,1,0:T(8,128)S(1)}, u32[]{:S(2)}) copy-start(f32[4,8,128,128]{3,2,1,0:T(8,128)S(1)} %fusion.1) | copy-start | bytes 6291460
  90.4 1.6 copy-start.4
  90.4 1.7 copy-start.11
  92.2 1.2 copy-start.10
  92.2 1.5 copy-start.15
  93.7 1.2 copy-start.5
  94.9 1.8 copy-start.8
  96.7 1.1 copy-start.2
  97.0 2.5 %copy-start.22 = (f32[512]{0:T(512)S(1)}, f32[512]{0:T(512)}, u32[]{:S(2)}) copy-start(f32[512]{0:T(512)} %param.28) | copy-start | bytes 6148
  97.0 2.6 %copy-start.13 = (bf16[128,2048]{1,0:T(8,128)(2,1)S(1)}, bf16[128,2048]{1,0:T(8,128)(2,1)}, u32[]{:S(2)}) copy-start(bf16[128,2048]{1,0:T(8,128)(2,1)} %copy-done.12) | copy-start | bytes 1572868
  98.7 66.4 %all-gather.5.cloned.1.call-start = ((), (), s32[]{:S(2)}) async-start(), calls=%async_computation.4 | async-start | bytes 3932160 | tf_op jit(solution)/shard_map/all_gather | solution.py:240
  99.4 104.0 %all-gather.7.cloned.1.call-start = ((), (), s32[]{:S(2)}) async-start(), calls=%async_computation.5 | async-start | bytes 2293760 | tf_op jit(solution)/shard_map/all_gather | solution.py:246
  101.3 6.0 %copy-start.7 = (f32[4,8,64,64]{3,2,1,0:T(8,128)S(1)}, f32[4,8,64,64]{3,2,1,0:T(8,128)}, u32[]{:S(2)}) copy-start(f32[4,8,64,64]{3,2,1,0:T(8,128)} %copy-done.6) | copy-start | bytes 1572868
  123.6 44.9 %copy-start.25 = (bf16[1,256,2048]{2,1,0:T(8,128)(2,1)S(1)}, bf16[1,256,2048]{2,1,0:T(8,128)(2,1)}, u32[]{:S(2)}) copy-start(bf16[1,256,2048]{2,1,0:T(8,128)(2,1)} %param.35) | copy-start | bytes 3145732
  165.1 3.4 %copy-start.24 = (bf16[768,2048]{1,0:T(8,128)(2,1)S(1)}, bf16[768,2048]{1,0:T(8,128)(2,1)}, u32[]{:S(2)}) copy-start(bf16[768,2048]{1,0:T(8,128)(2,1)} %all-gather.5.cloned.1.call-done) | copy-start | bytes 9437188
  169.5 6.1 %copy-start.3 = (f32[4,8,64,128]{3,2,1,0:T(8,128)S(1)}, f32[4,8,64,128]{3,2,1,0:T(8,128)}, u32[]{:S(2)}) copy-start(f32[4,8,64,128]{3,2,1,0:T(8,128)} %copy-done.2) | copy-start | bytes 3145732
  170.4 67.4 %reduce-scatter.2.cloned.1.call-start = ((), (), s32[]{:S(2)}) async-start(), calls=%async_computation.3 | async-start | bytes 1310720 | tf_op jit(solution)/shard_map/reduce_scatter | solution.py:173
  171.9 4.5 %copy-start.14 = (f32[4,8,64,128]{3,2,1,0:T(8,128)S(1)}, f32[4,8,64,128]{3,2,1,0:T(8,128)}, u32[]{:S(2)}) copy-start(f32[4,8,64,128]{3,2,1,0:T(8,128)} %convolution_subtract_fusion.6) | copy-start | bytes 3145732
  179.6 3.5 %copy-start.17 = (bf16[256,512]{1,0:T(8,128)(2,1)S(1)}, bf16[256,512]{1,0:T(8,128)(2,1)}, u32[]{:S(2)}) copy-start(bf16[256,512]{1,0:T(8,128)(2,1)} %param.22) | copy-start | bytes 786436
  179.6 3.5 %copy-start.21 = (f32[512]{0:T(512)S(1)}, f32[512]{0:T(512)}, u32[]{:S(2)}) copy-start(f32[512]{0:T(512)} %param.27) | copy-start | bytes 6148
  186.4 25.3 %copy-start.23 = (f32[128,4]{0,1:T(4,128)S(1)}, f32[128,4]{0,1:T(4,128)}, u32[]{:S(2)}) copy-start(f32[128,4]{0,1:T(4,128)} %param.32) | copy-start | bytes 6148
  186.4 25.5 %copy-start.19 = (s32[128,4]{0,1:T(4,128)S(1)}, s32[128,4]{0,1:T(4,128)}, u32[]{:S(2)}) copy-start(s32[128,4]{0,1:T(4,128)} %param.31) | copy-start | bytes 6148
  207.0 25.6 %all-to-all-start.1 = ((bf16[8,96,512]{2,1,0:T(8,128)(2,1)}), bf16[8,96,512]{2,1,0:T(8,128)(2,1)S(1)}, u32[]{:S(2)}, u32[]{:S(2)}) async-start(bf16[8,96,512]{2,1,0:T(8,128)(2,1)} %bitcast.187), calls=%async_computation.2 | async-start | bytes 1572864 | tf_op jit(solution)/shard_map/all_to_all | solution.py:255
Sparse Core Ops, SparseCore 0:
  98.8 21.1 all-gather.8
  121.8 43.2 all-gather.4
  170.5 32.8 all-gather.6
  206.7 27.9 reduce-scatter.1
where the time goes:
time: 246 us; the launch traced here: 244 us
  waiting for transfers between devices  109 us (44%)
  matrix products  54.7 us (22%)
  local copies, waits for them, and re-layouts  38.5 us (16%)
  other arithmetic  16.2 us (7%)
  between operations  14.6 us (6%)
  starting transfers between devices  11.6 us (5%)
    all_gather x1, waiting for transfers between devices, expert_exit(): pieces = lax.all_gather(flat_rows, 'tp', axis=1, tiled=True)  41.5 us
    dot_general x30, matrix products, product(): jnp.einsum(spec, left, right, precision=PRECISION, preferred_element_type...  32.6 us
    all_to_all x1, waiting for transfers between devices, expert_exit(): lax.all_to_all(routed_sum.astype(jnp.bfloat16).reshape(peer_count, slot_c...  20.5 us
    all_to_all x1, waiting for transfers between devices, expert_entry(): lax.all_to_all(own_slice, 'ep', split_axis=0, concat_axis=0, tiled=True)  20 us
    all_gather x1, waiting for transfers between devices, expert_exit(): lax.all_gather(jnp.concatenate([routed_hidden, shared_hidden], axis=1), '...  17 us
    reshape x6, local copies, waits for them, and re-layouts, by_block(): return matrix.astype(jnp.float32).reshape(block_count, span, head_count,...  12.3 us
    all_gather x1, waiting for transfers between devices, mixer_part(): everything = lax.all_gather(whole.astype(jnp.bfloat16), 'ep')  9.03 us
    all_to_all x1, starting transfers between devices, expert_entry(): lax.all_to_all(own_slice, 'ep', split_axis=0, concat_axis=0, tiled=True)  6.35 us
  transfers between devices with their start and end apart: 6, of which 5 were waited for; matrix products, arithmetic and copies ran while one was open for 17% of the time, Pallas kernels for 0%

commit v1 on v0

--- a/solution.py
+++ b/solution.py
@@ -237,7 +237,7 @@
     row_count, top_count = routing_output_weight.shape
     out_width = expert_down_weight.shape[2]
     flat_rows = arrived.reshape(-1, piece_width)
-    pieces = lax.all_gather(flat_rows, "tp", axis=1, tiled=True)
+    pieces = jnp.concatenate(lax.all_gather(flat_rows, "tp"), axis=1)
     gate_cols = expert_gate_weight[0]
     up_cols = expert_up_weight[0]
     pre_gate = jnp.einsum("fd,rd->fr", gate_cols, pieces, preferred_element_type=jnp.float32)

time: 246 us -> 250 us (1.016)
  local copies, waits for them, and re-layouts: 38.5 us -> 43.2 us
    all_gather x0 -> x1, local copies, waits for them, and re-layouts: none -> 4.66 us  [expert_exit(): pieces = jnp.concatenate(lax.all_gather(flat_rows, 'tp'), axis=1)]
  transfers between devices with their start and end apart: 6 -> 6, of which waited for: 5 -> 5; matrix products, arithmetic and copies ran while one was open for 17% -> 16% of each run, Pallas kernels for 0% -> 0%
where the time goes in v1:
time: 250 us; the launch traced here: 249 us
  waiting for transfers between devices  109 us (44%)
  matrix products  54.3 us (22%)
  local copies, waits for them, and re-layouts  43.2 us (17%)
  other arithmetic  16.2 us (6%)
  between operations  14.6 us (6%)
  starting transfers between devices  11.6 us (5%)
    all_gather x1, waiting for transfers between devices, expert_exit(): pieces = jnp.concatenate(lax.all_gather(flat_rows, 'tp'), axis=1)  41.6 us
    dot_general x30, matrix products, product(): jnp.einsum(spec, left, right, precision=PRECISION, preferred_element_type...  32.6 us
    all_to_all x1, waiting for transfers between devices, expert_exit(): lax.all_to_all(routed_sum.astype(jnp.bfloat16).reshape(peer_count, slot_c...  20.5 us
    all_to_all x1, waiting for transfers between devices, expert_entry(): lax.all_to_all(own_slice, 'ep', split_axis=0, concat_axis=0, tiled=True)  20 us
    all_gather x1, waiting for transfers between devices, expert_exit(): lax.all_gather(jnp.concatenate([routed_hidden, shared_hidden], axis=1), '...  17 us
    reshape x6, local copies, waits for them, and re-layouts, by_block(): return matrix.astype(jnp.float32).reshape(block_count, span, head_count,...  12.2 us
    all_gather x1, waiting for transfers between devices, mixer_part(): everything = lax.all_gather(whole.astype(jnp.bfloat16), 'ep')  9 us
    all_to_all x1, starting transfers between devices, expert_entry(): lax.all_to_all(own_slice, 'ep', split_axis=0, concat_axis=0, tiled=True)  6.35 us
  transfers between devices with their start and end apart: 6, of which 5 were waited for; matrix products, arithmetic and copies ran while one was open for 16% of the time, Pallas kernels for 0%

profile of v1, /device:TPU:0, one launch (start us, length us, event | category | flops | bytes accessed | tf_op | source)
XLA Modules:
  0.0 248.7 jit_solution(16187169213240984861)
XLA Ops:
  7.2 0.8 broadcast_multiply_fusion.2
  9.3 1.1 reduce-window.6
  10.8 2.4 scatter_custom_fusion
  13.3 1.2 fusion.32
  14.6 1.2 fusion.34
  16.7 4.3 %gather_fusion = bf16[768,2048]{1,0:T(8,128)(2,1)} fusion(bf16[129,2048]{1,0:T(8,128)(2,1)S(1)} %concatenate.33, s32[1024]{0:T(1024)S(1)} %pad_clamp_fusion.1), kind=kCustom, calls=%fused_computation | custom fusion | bytes 6294528 | tf_op jit(solution)/shard_map/jit(_take)/gather | solution.py:216
  21.0 2.3 dynamic-slice_select_fusion
  23.3 6.4 %all-to-all-start = ((bf16[8,96,512]{2,1,0:T(8,128)(2,1)}), bf16[8,96,512]{2,1,0:T(8,128)(2,1)S(1)}, u32[]{:S(2)}, u32[]{:S(2)}) async-start(bf16[8,96,512]{2,1,0:T(8,128)(2,1)} %dynamic-slice_select_fusion), calls=%async_computation | async-start | bytes 1572864 | tf_op jit(solution)/shard_map/all_to_all | solution.py:222
  30.6 20.0 %all-to-all-done = bf16[8,96,512]{2,1,0:T(8,128)(2,1)S(1)} async-done(((bf16[8,96,512]{2,1,0:T(8,128)(2,1)}), bf16[8,96,512]{2,1,0:T(8,128)(2,1)S(1)}, u32[]{:S(2)}, u32[]{:S(2)}) %all-to-all-start) | async-done | bytes 786464 | tf_op jit(solution)/shard_map/all_to_all | solution.py:222
  50.7 1.9 copy.339
  52.7 2.3 add_divide_fusion
  55.0 2.3 reshape.846
  57.2 1.4 reshape.889
  58.7 1.6 copy.345
  60.6 2.2 reshape.837
  62.8 2.4 reshape.888
  65.2 2.5 %copy.341 = f32[4,64,8,64]{3,1,2,0:T(8,128)} copy(f32[4,64,8,64]{1,0,3,2:T(4,128)} %reshape.888) | data formatting | bytes 1048576 | tf_op jit(solution)/shard_map/reshape | solution.py:95
  67.8 4.9 %fusion.67 = (f32[4,8,64,64]{3,2,1,0:T(8,128)S(1)}, f32[4,8,64,64]{3,2,1,0:T(8,128)S(1)}, f32[4,8,64,64]{3,2,1,0:T(8,128)S(1)}, f32[4,8,64,64]{3,2,1,0:T(8,128)S(1)}, f32[4,8,64,64]{3,2,1,0:T(8,128)}) fusion(f32[4,64,8,64]{3,2,1,0:T(8,128)} %reshape.846, f32[4,8,64]{2,1,0:T(8,128)S(1)} %add_rsqrt_fusion.1, f32[4,64,8,64]{3,1,2,0:T(8,128)S(1)} %copy.345, ...), kind=kOutput, calls=%fused_computation.114 | convolution fusion | flops 101715968 | bytes 4726784 | tf_op jit(solution)/shard_map/ts,nhsd->nhtd/dot_general | solution.py:105
  72.7 2.3 fusion.1
  75.0 1.0 fusion.64
  76.0 0.9 convolution_subtract_fusion.4
  76.9 0.8 fusion.62
  78.4 0.8 fusion.60
  79.9 0.8 fusion.58
  80.8 0.9 convolution_subtract_fusion.1
  81.7 0.8 fusion.56
  82.5 1.7 convolution_subtract_fusion
  84.2 1.6 slice_select_fusion.4
  85.8 2.1 reshape.839
  87.9 2.5 fusion.8
  90.4 1.2 fusion.129
  93.6 0.9 fusion.36
  94.9 1.7 convolution_subtract_fusion.5
  97.6 0.9 fusion.28
  99.4 1.7 convolution_bitcast_fusion.4
  101.2 2.0 fusion.31
  103.1 1.0 convert_multiply_fusion.2
  104.1 1.0 fusion
  105.1 2.1 copy.367
  107.2 3.7 %convolution_subtract_fusion.6 = f32[4,8,64,128]{3,2,1,0:T(8,128)} fusion(f32[4,8,64,128]{3,2,1,0:T(8,128)} %copy-done.8, f32[4,8,128,128]{3,2,1,0:T(8,128)} %copy-done.1, f32[4,8,64,64]{3,2,1,0:T(8,128)} %get-tuple-element.16, f32[4,8,64,64]{3,2,1,0:T(8,128)S(1)} %copy-done.7, pred[64,64]{1,0:T(8,128)(4,1)S(1)} %iota_compare_fusion.2), kind=kOutput, calls=%fused_computation.27 | convolution fusion | flops 101318656 | bytes 4722688 | tf_op jit(solution)/shard_map/nhts,nhsd->nhtd/dot_general | solution.py:47
  110.9 9.0 %all-gather.9.cloned.1.call-done = bf16[64,64,128]{2,1,0:T(8,128)(2,1)} async-done(((bf16[8,64,128]{2,1,0:T(8,128)(2,1)}), bf16[64,64,128]{2,1,0:T(8,128)(2,1)}) %all-gather.9.cloned.1.call-update) | async-done | bytes 1048592 | tf_op jit(solution)/shard_map/all_gather | solution.py:144
  119.9 1.2 fusion.27
  121.1 1.2 fusion.26
  122.3 1.2 fusion.25
  123.5 41.6 %all-gather.5.cloned.1.call-done = bf16[4,768,512]{2,1,0:T(8,128)(2,1)} async-done(((bf16[1,768,512]{2,1,0:T(8,128)(2,1)}), bf16[4,768,512]{2,1,0:T(8,128)(2,1)}) %all-gather.5.cloned.1.call-update) | async-done | bytes 3145744 | tf_op jit(solution)/shard_map/all_gather | solution.py:240
  165.1 4.7 %copy.370 = bf16[4,768,512]{1,2,0:T(8,128)(2,1)} copy(bf16[4,768,512]{2,1,0:T(8,128)(2,1)} %all-gather.5.cloned.1.call-done) | data formatting | bytes 6291456 | tf_op jit(solution)/shard_map/all_gather | solution.py:240
  169.8 3.1 %convolution_bitcast_fusion.2 = f32[256,768]{0,1:T(8,128)S(1)} fusion(bf16[768,2048]{0,1:T(8,128)(2,1)} %bitcast.182, bf16[1,256,2048]{2,1,0:T(8,128)(2,1)S(1)} %copy-done.25), kind=kOutput, calls=%fused_computation.32 | convolution fusion | flops 805306368 | bytes 4980736 | tf_op jit(solution)/shard_map/fd,rd->fr/dot_general | solution.py:243
  172.9 1.1 fusion.19
  175.1 1.2 fusion.24
  176.3 1.3 fusion.23
  177.6 1.2 fusion.22
  178.8 1.2 fusion.21
  180.8 1.0 fusion.130
  183.2 0.8 mul.191
  184.1 2.1 copy.366
  186.1 1.1 reshape.840
  187.6 3.2 %convolution_convert_fusion = bf16[256,2048]{1,0:T(8,128)(2,1)} fusion(bf16[512,2048]{1,0:T(8,128)(2,1)S(1)} %copy-done, bf16[256,512]{1,0:T(8,128)(2,1)} %param.25, f32[256,512]{1,0:T(8,128)} %copy.367, bf16[256,512]{1,0:T(8,128)(2,1)S(1)} %copy-done.18, f32[256,512]{1,0:T(8,128)} %copy.366, f32[256,512]{1,0:T(8,128)} %reshape.840, ...), kind=kOutput, calls=%fused_computation.4 | convolution fusion | flops 538574848 | bytes 5769216 | tf_op jit(solution)/shard_map/dot_general | solution.py:174
  190.9 17.0 %all-gather.7.cloned.1.call-done = bf16[1024,896]{0,1:T(8,128)(2,1)} async-done(((bf16[256,896]{0,1:T(8,128)(2,1)}), bf16[1024,896]{0,1:T(8,128)(2,1)}) %all-gather.7.cloned.1.call-update) | async-done | bytes 1835024 | tf_op jit(solution)/shard_map/all_gather | solution.py:246
  207.9 3.6 %fusion.14 = bf16[768,512]{1,0:T(8,128)(2,1)} fusion(bf16[1024,896]{0,1:T(8,128)(2,1)} %all-gather.7.cloned.1.call-done, bf16[1,1024,512]{2,1,0:T(8,128)(2,1)} %param.36), kind=kOutput, calls=%fused_computation.23 | convolution fusion | flops 805699584 | bytes 3407872 | tf_op jit(solution)/shard_map/fr,fd->rd/dot_general | solution.py:251
  211.4 4.6 %all-to-all-start.1 = ((bf16[8,96,512]{2,1,0:T(8,128)(2,1)}), bf16[8,96,512]{2,1,0:T(8,128)(2,1)S(1)}, u32[]{:S(2)}, u32[]{:S(2)}) async-start(bf16[8,96,512]{2,1,0:T(8,128)(2,1)} %bitcast.192), calls=%async_computation.2 | async-start | bytes 1572864 | tf_op jit(solution)/shard_map/all_to_all | solution.py:255
  216.5 20.5 %all-to-all-done.1 = bf16[8,96,512]{2,1,0:T(8,128)(2,1)S(1)} async-done(((bf16[8,96,512]{2,1,0:T(8,128)(2,1)}), bf16[8,96,512]{2,1,0:T(8,128)(2,1)S(1)}, u32[]{:S(2)}, u32[]{:S(2)}) %all-to-all-start.1) | async-done | bytes 786464 | tf_op jit(solution)/shard_map/all_to_all | solution.py:255
  237.0 2.0 gather_fusion.1
  239.1 0.9 multiply_reduce_fusion
  239.9 2.3 fusion.29
  (134 shorter events, 13.6 us)
Async XLA Ops:
  7.2 180.4 %copy-start = (bf16[512,2048]{1,0:T(8,128)(2,1)S(1)}, bf16[512,2048]{1,0:T(8,128)(2,1)}, u32[]{:S(2)}) copy-start(bf16[512,2048]{1,0:T(8,128)(2,1)} %param.29) | copy-start | bytes 6291460
  15.8 0.8 copy-start.12
  21.0 29.6 %copy-start.19 = (bf16[256,512]{1,0:T(8,128)(2,1)S(1)}, bf16[256,512]{1,0:T(8,128)(2,1)}, u32[]{:S(2)}) copy-start(bf16[256,512]{1,0:T(8,128)(2,1)} %param.21) | copy-start | bytes 786436
  21.0 31.7 %copy-start.21 = (f32[512]{0:T(512)S(1)}, f32[512]{0:T(512)}, u32[]{:S(2)}) copy-start(f32[512]{0:T(512)} %param.26) | copy-start | bytes 6148
  23.3 27.3 %all-to-all-start = ((bf16[8,96,512]{2,1,0:T(8,128)(2,1)}), bf16[8,96,512]{2,1,0:T(8,128)(2,1)S(1)}, u32[]{:S(2)}, u32[]{:S(2)}) async-start(bf16[8,96,512]{2,1,0:T(8,128)(2,1)} %dynamic-slice_select_fusion), calls=%async_computation | async-start | bytes 1572864 | tf_op jit(solution)/shard_map/all_to_all | solution.py:222
  29.7 90.2 %all-gather.9.cloned.1.call-start = ((), (), s32[]{:S(2)}) async-start(), calls=%async_computation.6 | async-start | bytes 1179648 | tf_op jit(solution)/shard_map/all_gather | solution.py:144
  50.6 6.6 %copy-start.17 = (bf16[8,96,512]{2,1,0:T(8,128)(2,1)}, bf16[8,96,512]{2,1,0:T(8,128)(2,1)S(1)}, u32[]{:S(2)}) copy-start(bf16[8,96,512]{2,1,0:T(8,128)(2,1)S(1)} %all-to-all-done) | copy-start | bytes 2359300
  72.7 2.3 copy-start.6
  72.7 2.3 copy-start.9
  75.0 9.2 %copy-start.1 = (f32[4,8,128,128]{3,2,1,0:T(8,128)}, f32[4,8,128,128]{3,2,1,0:T(8,128)S(1)}, u32[]{:S(2)}) copy-start(f32[4,8,128,128]{3,2,1,0:T(8,128)S(1)} %fusion.1) | copy-start | bytes 6291460
  90.4 1.6 copy-start.4
  90.4 1.7 copy-start.11
  92.1 1.2 copy-start.10
  92.1 1.5 copy-start.15
  93.6 1.2 copy-start.5
  94.9 1.8 copy-start.8
  96.6 1.0 copy-start.2
  96.9 2.4 copy-start.23
  96.9 2.5 %copy-start.13 = (bf16[128,2048]{1,0:T(8,128)(2,1)S(1)}, bf16[128,2048]{1,0:T(8,128)(2,1)}, u32[]{:S(2)}) copy-start(bf16[128,2048]{1,0:T(8,128)(2,1)} %copy-done.12) | copy-start | bytes 1572868
  98.5 66.6 %all-gather.5.cloned.1.call-start = ((), (), s32[]{:S(2)}) async-start(), calls=%async_computation.4 | async-start | bytes 3932160 | tf_op jit(solution)/shard_map/all_gather | solution.py:240
  99.3 108.6 %all-gather.7.cloned.1.call-start = ((), (), s32[]{:S(2)}) async-start(), calls=%async_computation.5 | async-start | bytes 2293760 | tf_op jit(solution)/shard_map/all_gather | solution.py:246
  101.1 6.0 %copy-start.7 = (f32[4,8,64,64]{3,2,1,0:T(8,128)S(1)}, f32[4,8,64,64]{3,2,1,0:T(8,128)}, u32[]{:S(2)}) copy-start(f32[4,8,64,64]{3,2,1,0:T(8,128)} %copy-done.6) | copy-start | bytes 1572868
  123.5 46.3 %copy-start.25 = (bf16[1,256,2048]{2,1,0:T(8,128)(2,1)S(1)}, bf16[1,256,2048]{2,1,0:T(8,128)(2,1)}, u32[]{:S(2)}) copy-start(bf16[1,256,2048]{2,1,0:T(8,128)(2,1)} %param.34) | copy-start | bytes 3145732
  169.8 3.1 %copy-start.16 = (bf16[4,768,512]{1,2,0:T(8,128)(2,1)S(1)}, bf16[4,768,512]{1,2,0:T(8,128)(2,1)}, u32[]{:S(2)}) copy-start(bf16[4,768,512]{1,2,0:T(8,128)(2,1)} %copy.370) | copy-start | bytes 9437188
  169.8 3.1 %copy-start.26 = (bf16[1,256,2048]{2,1,0:T(8,128)(2,1)S(1)}, bf16[1,256,2048]{2,1,0:T(8,128)(2,1)}, u32[]{:S(2)}) copy-start(bf16[1,256,2048]{2,1,0:T(8,128)(2,1)} %param.35) | copy-start | bytes 3145732
  174.0 6.1 %copy-start.3 = (f32[4,8,64,128]{3,2,1,0:T(8,128)S(1)}, f32[4,8,64,128]{3,2,1,0:T(8,128)}, u32[]{:S(2)}) copy-start(f32[4,8,64,128]{3,2,1,0:T(8,128)} %copy-done.2) | copy-start | bytes 3145732
  174.8 67.4 %reduce-scatter.2.cloned.1.call-start = ((), (), s32[]{:S(2)}) async-start(), calls=%async_computation.3 | async-start | bytes 1310720 | tf_op jit(solution)/shard_map/reduce_scatter | solution.py:173
  176.3 4.5 %copy-start.14 = (f32[4,8,64,128]{3,2,1,0:T(8,128)S(1)}, f32[4,8,64,128]{3,2,1,0:T(8,128)}, u32[]{:S(2)}) copy-start(f32[4,8,64,128]{3,2,1,0:T(8,128)} %convolution_subtract_fusion.6) | copy-start | bytes 3145732
  184.1 3.5 %copy-start.18 = (bf16[256,512]{1,0:T(8,128)(2,1)S(1)}, bf16[256,512]{1,0:T(8,128)(2,1)}, u32[]{:S(2)}) copy-start(bf16[256,512]{1,0:T(8,128)(2,1)} %param.22) | copy-start | bytes 786436
  184.1 3.5 %copy-start.22 = (f32[512]{0:T(512)S(1)}, f32[512]{0:T(512)}, u32[]{:S(2)}) copy-start(f32[512]{0:T(512)} %param.27) | copy-start | bytes 6148
  190.8 25.3 %copy-start.24 = (f32[128,4]{0,1:T(4,128)S(1)}, f32[128,4]{0,1:T(4,128)}, u32[]{:S(2)}) copy-start(f32[128,4]{0,1:T(4,128)} %param.32) | copy-start | bytes 6148
  190.8 25.5 %copy-start.20 = (s32[128,4]{0,1:T(4,128)S(1)}, s32[128,4]{0,1:T(4,128)}, u32[]{:S(2)}) copy-start(s32[128,4]{0,1:T(4,128)} %param.31) | copy-start | bytes 6148
  211.4 25.6 %all-to-all-start.1 = ((bf16[8,96,512]{2,1,0:T(8,128)(2,1)}), bf16[8,96,512]{2,1,0:T(8,128)(2,1)S(1)}, u32[]{:S(2)}, u32[]{:S(2)}) async-start(bf16[8,96,512]{2,1,0:T(8,128)(2,1)} %bitcast.192), calls=%async_computation.2 | async-start | bytes 1572864 | tf_op jit(solution)/shard_map/all_to_all | solution.py:255
Sparse Core Ops, SparseCore 0:
  98.7 21.1 all-gather.8
  121.7 43.3 all-gather.4
  174.9 32.8 all-gather.6
  211.2 27.9 reduce-scatter.1
